TPU v7x, 32 devices: a whole 2x2x4 slice. The times are simulated.
32 devices in a mesh: ep: 16 (over z, y, x), tp: 2 (over core).
Axes of the slice: x: 2, y: 2, z: 4, core: 2. Of those that a mesh axis runs over, the one named last changes fastest.
Arguments:
- resid: bfloat16 [256, 2048], P('ep'), may hold values from -6 to 6
- proj_x: bfloat16 [256, 2048], P('ep', 'tp'), may hold values from -6 to 6
- proj_z: bfloat16 [256, 2048], P('ep', 'tp'), may hold values from -6 to 6
- proj_bc: bfloat16 [256, 2, 512], P('ep', None, 'tp'), may hold values from -6 to 6
- proj_dt: bfloat16 [256, 32], P('ep', 'tp'), may hold values from -6 to 6
- tail_x: bfloat16 [256, 3, 2048], P('ep', None, 'tp'), may hold values from -6 to 6
- tail_bc: bfloat16 [256, 3, 2, 512], P('ep', None, None, 'tp'), may hold values from -6 to 6
- taps_x: bfloat16 [4, 2048], P(None, 'tp'), may hold values from -3 to 3
- taps_bc: bfloat16 [4, 2, 512], P(None, None, 'tp'), may hold values from -3 to 3
- ssm_state: float32 [256, 32, 4096], P('ep', 'tp'), may hold values from -1.5 to 1.5
- dt_bias: float32 [32], P('tp'), may hold values from -4 to 0
- decay_log: float32 [32], P('tp'), may hold values from -1 to 2.5
- group_gain: float32 [2048], P('tp'), may hold values from 0.1 to 1.9
- out_proj: bfloat16 [2048, 2048], P('tp', 'ep'), may hold values from -0.125 to 0.125
- ffn_gain: float32 [2048], replicated, may hold values from 0.1 to 1.9
- dense_gate: bfloat16 [2048, 4096], P(None, ('ep', 'tp')), may hold values from -0.125 to 0.125
- dense_up: bfloat16 [2048, 4096], P(None, ('ep', 'tp')), may hold values from -0.125 to 0.125
- dense_down: bfloat16 [4096, 2048], P(('ep', 'tp')), may hold values from -0.09375 to 0.09375
- branch_gate: bfloat16 [2048], replicated, may hold values from -0.125 to 0.125
- group_weights: float32 [256, 4], replicated, may hold values from 0.2 to 1
- expert_ids: int32 [256, 6], replicated, may hold values from 0 to 15, all different within a row; in each aligned block of 16 rows (0 to 15, 16 to 31, ...) at most 7 rows name the same one
- expert_weights: float32 [256, 6], replicated, may hold values from 0.1 to 1
- exp_gate: bfloat16 [16, 2048, 512], P('ep', None, 'tp'), may hold values from -0.125 to 0.125
- exp_up: bfloat16 [16, 2048, 512], P('ep', None, 'tp'), may hold values from -0.125 to 0.125
- exp_down: bfloat16 [16, 512, 2048], P('ep', 'tp'), may hold values from -0.25 to 0.25
Outputs:
- out: bfloat16 [256, 2048], P(('ep', 'tp'))
- new_state: float32 [256, 32, 4096], P('ep', 'tp')
Inputs may be any that keep to these rules, and one draw needn't show every extreme that they name: `expert_ids`: each row names 6 different experts. In the rows of one index of ep (aligned blocks of 16 rows) no expert is named more than 7 times, a bound that some block reaches.
All inputs are finite; a program needn't handle non-finite values.
Results may differ from a plain program's by a relative error of at most 0.013.
Values may be sent and summed in bfloat16 or wider, within the bound.
A program may use at most 128 MiB of HBM per device.

v0:
```python
import jax
import jax.numpy as jnp
from jax import lax
from jax.sharding import PartitionSpec as P

HEAD_P = 64
NSTATE = 64
GROUPS = 4
TOPK = 6
HPG = 4
EPSILON = 1e-06


def state_update(
    proj_x,
    proj_z,
    proj_bc,
    proj_dt,
    tail_x,
    tail_bc,
    taps_x,
    taps_bc,
    ssm_state,
    dt_bias,
    decay_log,
    group_gain,
):
    window_x = jnp.concatenate([tail_x, proj_x[:, None]], axis=1).astype(jnp.float32)
    conv_x = jax.nn.silu(jnp.sum(window_x * taps_x.astype(jnp.float32)[None], axis=1))
    window_bc = jnp.concatenate([tail_bc, proj_bc[:, None]], axis=1).astype(jnp.float32)
    conv_bc = jax.nn.silu(jnp.sum(window_bc * taps_bc.astype(jnp.float32)[None], axis=1))
    count = proj_x.shape[0]
    heads = proj_dt.shape[1]
    x_heads = conv_x.reshape(count, heads, HEAD_P)
    grouped_bc = conv_bc.reshape(count, 2, heads // HPG, NSTATE)
    input_heads = jnp.repeat(grouped_bc[:, 0], HPG, axis=1)
    read_heads = jnp.repeat(grouped_bc[:, 1], HPG, axis=1)
    step_size = jax.nn.softplus(proj_dt.astype(jnp.float32) + dt_bias)
    decay = jnp.exp(-step_size * jnp.exp(decay_log))
    state = ssm_state.reshape(count, heads, HEAD_P, NSTATE)
    fresh = (step_size[:, :, None] * x_heads)[:, :, :, None] * input_heads[:, :, None, :]
    new_state = decay[:, :, None, None] * state + fresh
    readout = jnp.sum(new_state * read_heads[:, :, None, :], axis=-1)
    gated = readout.reshape(count, heads * HEAD_P) * jax.nn.silu(proj_z.astype(jnp.float32))
    grouped = gated.reshape(count, heads // HPG, HPG * HEAD_P)
    grouped = grouped * lax.rsqrt(jnp.mean(grouped * grouped, axis=-1, keepdims=True) + EPSILON)
    y_out = (grouped.reshape(count, heads * HEAD_P) * group_gain).astype(jnp.bfloat16)
    return (y_out, new_state.reshape(count, heads, HEAD_P * NSTATE))


def shards(
    resid,
    proj_x,
    proj_z,
    proj_bc,
    proj_dt,
    tail_x,
    tail_bc,
    taps_x,
    taps_bc,
    ssm_state,
    dt_bias,
    decay_log,
    group_gain,
    out_proj,
    ffn_gain,
    dense_gate,
    dense_up,
    dense_down,
    branch_gate,
    group_weights,
    expert_ids,
    expert_weights,
    exp_gate,
    exp_up,
    exp_down,
):
    y_out, new_state = state_update(
        proj_x,
        proj_z,
        proj_bc,
        proj_dt,
        tail_x,
        tail_bc,
        taps_x,
        taps_bc,
        ssm_state,
        dt_bias,
        decay_log,
        group_gain,
    )
    partial_value = jnp.dot(
        lax.all_gather(y_out, "ep", axis=0, tiled=True),
        out_proj,
        preferred_element_type=jnp.float32,
    )
    partial_value = lax.all_to_all(
        partial_value.astype(jnp.bfloat16), "ep", split_axis=0, concat_axis=1, tiled=True
    ).astype(partial_value.dtype)
    mixed = lax.psum(partial_value.astype(jnp.bfloat16), "tp").astype(jnp.float32)
    resid_new = (resid.astype(jnp.float32) + mixed).astype(jnp.bfloat16)
    widened = resid_new.astype(jnp.float32)
    normed = (
        widened
        * lax.rsqrt(jnp.mean(widened * widened, axis=-1, keepdims=True) + EPSILON)
        * ffn_gain
    ).astype(jnp.bfloat16)
    gathered = lax.all_gather(normed, "ep", axis=0, tiled=True)
    score = jnp.dot(gathered, branch_gate, preferred_element_type=jnp.float32)
    dense_pre = jnp.dot(gathered, dense_gate, preferred_element_type=jnp.float32)
    dense_lin = jnp.dot(gathered, dense_up, preferred_element_type=jnp.float32)
    dense_hidden = (jax.nn.sigmoid(score)[:, None] * jax.nn.silu(dense_pre) * dense_lin).astype(
        jnp.bfloat16
    )
    experts = lax.axis_size("ep")
    expert_own = lax.axis_index("ep")
    cores = lax.axis_size("tp")
    core_index = lax.axis_index("tp")
    batch = gathered.shape[0]
    rows_each = batch // experts
    half_rows = rows_each // cores
    pairs = rows_each * TOPK
    capacity = (pairs + experts - 1) // experts + 1
    group_size = experts // GROUPS
    levels = jnp.arange(1, capacity + 1, dtype=jnp.int32)
    pair_row = jnp.arange(pairs, dtype=jnp.int32) // TOPK
    pick = (jnp.arange(GROUPS, dtype=jnp.int32) == expert_own // group_size).astype(jnp.float32)
    coarse = jnp.sum(group_weights * pick[None], axis=1)
    pair_weight = (expert_weights * coarse[:, None]).reshape(experts, pairs)
    hits = (expert_ids.reshape(experts, pairs) == expert_own).astype(jnp.int32)
    ranks = jnp.cumsum(hits, axis=1, dtype=jnp.int32)
    select = hits[:, None, :] * (ranks[:, None, :] == levels[None, :, None]).astype(jnp.int32)
    local_row = jnp.sum(select * pair_row[None, None, :], axis=-1, dtype=jnp.int32)
    filled = jnp.sum(select, axis=-1, dtype=jnp.int32).reshape(-1)
    slot_weight = jnp.sum(select.astype(jnp.float32) * pair_weight[:, None, :], axis=-1).reshape(-1)
    row_index = (local_row + jnp.arange(experts, dtype=jnp.int32)[:, None] * rows_each).reshape(-1)
    slot_rows = jnp.take(gathered, row_index, axis=0)
    slot_pre = jnp.dot(slot_rows, exp_gate[0], preferred_element_type=jnp.float32)
    slot_lin = jnp.dot(slot_rows, exp_up[0], preferred_element_type=jnp.float32)
    slot_hidden = (slot_weight[:, None] * jax.nn.silu(slot_pre) * slot_lin).astype(jnp.bfloat16)
    placing = (jnp.arange(batch, dtype=jnp.int32)[:, None] == row_index[None, :]) & (
        filled[None, :] > 0
    )
    row_hidden = jnp.dot(
        placing.astype(jnp.bfloat16), slot_hidden, preferred_element_type=jnp.float32
    ).astype(jnp.bfloat16)
    joined = jnp.concatenate([dense_hidden, row_hidden], axis=1)
    down_all = jnp.concatenate([dense_down, exp_down[0]], axis=0)
    inner_width = joined.shape[1]
    ordered = (
        joined.reshape(experts, cores, half_rows, inner_width)
        .transpose(1, 0, 2, 3)
        .reshape(batch, inner_width)
    )
    halved = lax.psum_scatter(
        jnp.dot(ordered, down_all, preferred_element_type=jnp.float32).astype(jnp.bfloat16),
        "tp",
        scatter_dimension=0,
        tiled=True,
    ).astype(jnp.float32)
    branch = lax.psum_scatter(halved, "ep", scatter_dimension=0, tiled=True)
    own_rows = lax.dynamic_slice_in_dim(widened, core_index * half_rows, half_rows, 0)
    out = (own_rows + branch).astype(jnp.bfloat16)
    return (out, new_state)


def solution(mesh):
    return jax.shard_map(
        shards,
        mesh=mesh,
        in_specs=(
            P("ep", None),
            P("ep", "tp"),
            P("ep", "tp"),
            P("ep", None, "tp"),
            P("ep", "tp"),
            P("ep", None, "tp"),
            P("ep", None, None, "tp"),
            P(None, "tp"),
            P(None, None, "tp"),
            P("ep", "tp", None),
            P("tp"),
            P("tp"),
            P("tp"),
            P("tp", "ep"),
            P(),
            P(None, ("ep", "tp")),
            P(None, ("ep", "tp")),
            P(("ep", "tp"), None),
            P(),
            P(),
            P(),
            P(),
            P("ep", None, "tp"),
            P("ep", None, "tp"),
            P("ep", "tp", None),
        ),
        out_specs=(P(("ep", "tp"), None), P("ep", "tp", None)),
        check_vma=False,
    )
```

profile of v0, /device:TPU:0, one launch (start us, length us, event | category | flops | bytes accessed | tf_op | source)
XLA Modules:
  0.0 270.5 jit_solution(9776574114942145212)
XLA Ops:
  7.2 0.0 copy-start
  7.2 0.7 exp.39
  7.9 0.7 convert_element_type.90
  8.6 0.9 multiply_reduce_fusion.3
  9.6 0.1 reduce_sum.88
  9.7 0.7 convert_element_type.88
  10.4 0.9 multiply_reduce_fusion.1
  11.4 0.1 reduce_sum.86
  11.5 7.9 %reshape.179 = f32[16,16,64,64]{3,2,1,0:T(8,128)} reshape(f32[16,16,4096]{2,1,0:T(8,128)} %param.34) | data formatting | bytes 8388608 | tf_op jit(solution)/shard_map/reshape | solution.py:40
  19.4 0.1 multiply_multiply_fusion
  19.6 0.0 copy-start.5
  19.6 0.0 copy-start.7
  19.6 0.0 copy-start.4
  19.7 0.0 copy-start.8
  19.7 8.5 %broadcast_multiply_fusion = (f32[16,16,64,64]{3,2,1,0:T(8,128)}, f32[16,16,64]{2,1,0:T(8,128)S(1)}) fusion(f32[16,16,64]{2,1,0:T(8,128)S(1)} %bitcast.44, f32[16,16,64]{2,1,0:T(8,128)S(1)} %multiply_multiply_fusion, f32[16,16,64]{2,1,0:T(8,128)S(1)} %bitcast.45, f32[16,16,64,64]{3,2,1,0:T(8,128)} %reshape.179, f32[16,16]{1,0:T(8,128)S(1)} %get-tuple-element.11), kind=kLoop, calls=%fused_computation.3 | loop fusion | flops 5226496 | bytes 8651776 | tf_op jit(solution)/shard_map/mul | solution.py:41
  28.2 0.1 reshape.180
  28.4 0.1 reduce_sum.90
  28.5 0.1 mul.250
  28.7 45.3 %all_gather.6 = bf16[256,1024]{1,0:T(8,128)(2,1)S(1)} all-gather(bf16[16,1024]{1,0:T(8,128)(2,1)S(1)} %multiply_convert_fusion.1), channel_id=1, replica_groups=mesh['ep'=16,'tp'=2] {'ep'}, dimensions={0}, use_global_device_ids=true | all-gather | bytes 557056 | tf_op jit(solution)/shard_map/all_gather | solution.py:93
  74.0 0.9 convolution_convert_fusion.2
  74.9 3.5 %all-to-all-start = ((bf16[16,16,128]{2,1,0:T(8,128)(2,1)}), bf16[16,16,128]{2,1,0:T(8,128)(2,1)S(1)}, u32[]{:S(2)}, u32[]{:S(2)}) async-start(bf16[16,16,128]{2,1,0:T(8,128)(2,1)} %bitcast.6), calls=%async_computation | async-start | bytes 131072 | tf_op jit(solution)/shard_map/all_to_all | solution.py:97
  78.4 0.0 all-reduce.2.cloned.1.call-start
  78.5 7.4 %all-to-all-done = bf16[16,16,128]{2,1,0:T(8,128)(2,1)S(1)} async-done(((bf16[16,16,128]{2,1,0:T(8,128)(2,1)}), bf16[16,16,128]{2,1,0:T(8,128)(2,1)S(1)}, u32[]{:S(2)}, u32[]{:S(2)}) %all-to-all-start) | async-done | bytes 65568 | tf_op jit(solution)/shard_map/all_to_all | solution.py:97
  85.9 0.6 copy_bitcast_fusion
  86.6 0.0 all-reduce.2.cloned.1.call-update
  86.6 0.0 all-gather.2.cloned.1.call-start
  86.7 14.5 %all-reduce.2.cloned.1.call-done = bf16[16,2048]{1,0:T(8,128)(2,1)} async-done(((bf16[16,2048]{1,0:T(8,128)(2,1)}), bf16[16,2048]{1,0:T(8,128)(2,1)}) %all-reduce.2.cloned.1.call-update) | async-done | bytes 65552 | tf_op jit(solution)/shard_map/psum | solution.py:100
  101.2 1.0 fusion.21
  102.1 1.6 multiply_convert_fusion
  103.7 0.0 all-gather.2.cloned.1.call-update
  103.7 0.0 reduce-scatter.3.cloned.1.call-start
  103.8 0.1 copy.39
  103.9 0.1 reshape.183
  104.0 0.3 reduce_window_sum.11
  104.3 0.4 select_reduce_fusion
  104.7 0.1 copy.40
  104.8 0.1 add.162
  104.9 0.1 add.159
  105.0 0.1 multiply_reduce_fusion.4
  105.1 0.1 copy.42
  105.2 0.1 mul.274
  105.4 0.2 fusion.26
  105.5 0.1 copy.43
  105.6 0.1 mul.277
  105.7 0.1 copy.41
  105.8 0.1 gt.18
  106.0 54.8 %all-gather.2.cloned.1.call-done = bf16[256,2048]{1,0:T(8,128)(2,1)} async-done(((bf16[16,2048]{1,0:T(8,128)(2,1)}), bf16[256,2048]{1,0:T(8,128)(2,1)}) %all-gather.2.cloned.1.call-update) | async-done | bytes 1048592 | tf_op jit(solution)/shard_map/all_gather | solution.py:108
  160.8 1.6 fusion.36
  162.4 2.8 %gather_fusion = bf16[112,2048]{1,0:T(8,128)(2,1)S(1)} fusion(bf16[256,2048]{1,0:T(8,128)(2,1)} %all-gather.2.cloned.1.call-done, s32[1024]{0:T(1024)S(1)} %pad_clamp_fusion), kind=kCustom, calls=%fused_computation | custom fusion | bytes 917952 | tf_op jit(solution)/shard_map/jit(_take)/gather | solution.py:137
  165.3 1.6 fusion.7
  166.8 0.6 convolution_convert_fusion.1
  167.5 0.5 fusion.37
  168.0 1.5 fusion.3
  169.5 0.2 copy.45
  169.7 3.0 %convolution_convert_fusion = bf16[256,2048]{1,0:T(8,128)(2,1)} fusion(bf16[256,384]{1,0:T(8,128)(2,1)S(1)} %bitcast.48, bf16[256,2048]{1,0:T(8,128)(2,1)} %bitcast.52, bf16[128,2048]{1,0:T(8,128)(2,1)} %param.42), kind=kOutput, calls=%fused_computation.4 | convolution fusion | flops 406323200 | bytes 2818048 | tf_op jit(solution)/shard_map/dot_general | solution.py:156
  172.8 0.0 reduce-scatter.3.cloned.1.call-update
  172.8 0.0 reduce-scatter.5.cloned.1.call-start
  172.8 7.3 %reduce-scatter.3.cloned.1.call-done = bf16[128,2048]{1,0:T(8,128)(2,1)} async-done(((bf16[256,2048]{1,0:T(8,128)(2,1)}), bf16[128,2048]{1,0:T(8,128)(2,1)}) %reduce-scatter.3.cloned.1.call-update) | async-done | bytes 524304 | tf_op jit(solution)/shard_map/reduce_scatter | solution.py:155
  180.2 2.2 convert_element_type.106
  182.4 0.0 reduce-scatter.5.cloned.1.call-update
  182.4 7.9 %mul.284 = f32[16,16,4096]{2,1,0:T(8,128)} reshape(f32[16,16,64,64]{3,2,1,0:T(8,128)} %get-tuple-element.4) | data formatting | bytes 8388608 | tf_op jit(solution)/shard_map/mul | solution.py:41
  190.3 6.6 %multiply_add_fusion = f32[16,16,4096]{2,1,0:T(8,128)} fusion(f32[16,16,4096]{2,1,0:T(8,128)} %mul.284, f32[16,16,4096]{2,1,0:T(8,128)} %param.34, f32[16,16]{1,0:T(8,128)S(1)} %get-tuple-element.11), kind=kLoop, calls=%fused_computation.2 | loop fusion | flops 2097152 | bytes 12583936 | tf_op jit(solution)/shard_map/add | solution.py:42
  196.9 65.7 %reduce-scatter.5.cloned.1.call-done = f32[8,2048]{1,0:T(8,128)} async-done(((f32[128,2048]{1,0:T(8,128)}), f32[8,2048]{1,0:T(8,128)}) %reduce-scatter.5.cloned.1.call-update) | async-done | bytes 65552 | tf_op jit(solution)/shard_map/reduce_scatter | solution.py:161
  262.5 1.5 add_convert_fusion.1
  (49 shorter events, 0.4 us)
Async XLA Ops:
  7.2 159.7 %copy-start = (bf16[1,2048,256]{2,1,0:T(8,128)(2,1)S(1)}, bf16[1,2048,256]{2,1,0:T(8,128)(2,1)}, u32[]{:S(2)}) copy-start(bf16[1,2048,256]{2,1,0:T(8,128)(2,1)} %param.48) | copy-start | bytes 3145732
  11.5 7.9 %copy-start.12 = (bf16[16,16]{1,0:T(8,128)(2,1)S(1)}, bf16[16,16]{1,0:T(8,128)(2,1)}, u32[]{:S(2)}) copy-start(bf16[16,16]{1,0:T(8,128)(2,1)} %param.29) | copy-start | bytes 1540
  11.5 7.9 %copy-start.13 = (f32[16]{0:T(128)S(1)}, f32[16]{0:T(128)}, u32[]{:S(2)}) copy-start(f32[16]{0:T(128)} %param.35) | copy-start | bytes 196
  19.6 8.7 %copy-start.5 = (bf16[16,1024]{1,0:T(8,128)(2,1)S(1)}, bf16[16,1024]{1,0:T(8,128)(2,1)}, u32[]{:S(2)}) copy-start(bf16[16,1024]{1,0:T(8,128)(2,1)} %param.27) | copy-start | bytes 98308
  19.6 9.0 %copy-start.9 = (f32[1024]{0:T(1024)S(1)}, f32[1024]{0:T(1024)}, u32[]{:S(2)}) copy-start(f32[1024]{0:T(1024)} %param.37) | copy-start | bytes 12292
  19.6 54.4 %copy-start.3 = (bf16[1024,128]{1,0:T(8,128)(2,1)S(1)}, bf16[1024,128]{1,0:T(8,128)(2,1)}, u32[]{:S(2)}) copy-start(bf16[1024,128]{1,0:T(8,128)(2,1)} %param.38) | copy-start | bytes 786436
  19.6 67.0 %copy-start.7 = (s32[256,6]{0,1:T(8,128)S(1)}, s32[256,6]{0,1:T(8,128)}, u32[]{:S(2)}) copy-start(s32[256,6]{0,1:T(8,128)} %param.45) | copy-start | bytes 18436
  19.6 81.5 %copy-start.4 = (bf16[16,2048]{1,0:T(8,128)(2,1)S(1)}, bf16[16,2048]{1,0:T(8,128)(2,1)}, u32[]{:S(2)}) copy-start(bf16[16,2048]{1,0:T(8,128)(2,1)} %param.25) | copy-start | bytes 196612
  19.6 82.5 %copy-start.6 = (f32[2048]{0:T(1024)S(1)}, f32[2048]{0:T(1024)}, u32[]{:S(2)}) copy-start(f32[2048]{0:T(1024)} %param.39) | copy-start | bytes 24580
  19.7 85.3 %copy-start.11 = (f32[256,4]{0,1:T(4,128)S(1)}, f32[256,4]{0,1:T(4,128)}, u32[]{:S(2)}) copy-start(f32[256,4]{0,1:T(4,128)} %param.44) | copy-start | bytes 12292
  19.7 85.4 %copy-start.8 = (f32[256,6]{0,1:T(8,128)S(1)}, f32[256,6]{0,1:T(8,128)}, u32[]{:S(2)}) copy-start(f32[256,6]{0,1:T(8,128)} %param.46) | copy-start | bytes 18436
  19.7 86.2 %copy-start.10 = (bf16[2048]{0:T(1024)(128)(2,1)S(1)}, bf16[2048]{0:T(1024)(128)(2,1)}, u32[]{:S(2)}) copy-start(bf16[2048]{0:T(1024)(128)(2,1)} %param.43) | copy-start | bytes 12292
  74.9 11.0 %all-to-all-start = ((bf16[16,16,128]{2,1,0:T(8,128)(2,1)}), bf16[16,16,128]{2,1,0:T(8,128)(2,1)S(1)}, u32[]{:S(2)}, u32[]{:S(2)}) async-start(bf16[16,16,128]{2,1,0:T(8,128)(2,1)} %bitcast.6), calls=%async_computation | async-start | bytes 131072 | tf_op jit(solution)/shard_map/all_to_all | solution.py:97
  78.4 22.7 %all-reduce.2.cloned.1.call-start = ((), (), s32[]{:S(2)}) async-start(), calls=%async_computation.3 | async-start | bytes 131072 | tf_op jit(solution)/shard_map/psum | solution.py:100
  86.6 74.2 %all-gather.2.cloned.1.call-start = ((), (), s32[]{:S(2)}) async-start(), calls=%async_computation.4 | async-start | bytes 1114112 | tf_op jit(solution)/shard_map/all_gather | solution.py:108
  103.7 76.4 %reduce-scatter.3.cloned.1.call-start = ((), (), s32[]{:S(2)}) async-start(), calls=%async_computation.5 | async-start | bytes 1572864 | tf_op jit(solution)/shard_map/reduce_scatter | solution.py:155
  162.4 5.0 %copy-start.1 = (bf16[256,2048]{1,0:T(8,128)(2,1)S(1)}, bf16[256,2048]{1,0:T(8,128)(2,1)}, u32[]{:S(2)}) copy-start(bf16[256,2048]{1,0:T(8,128)(2,1)} %all-gather.2.cloned.1.call-done) | copy-start | bytes 3145732
  162.4 5.1 %copy-start.2 = (bf16[2048,128]{1,0:T(8,128)(2,1)S(1)}, bf16[2048,128]{1,0:T(8,128)(2,1)}, u32[]{:S(2)}) copy-start(bf16[2048,128]{1,0:T(8,128)(2,1)} %param.40) | copy-start | bytes 1572868
  172.8 89.7 %reduce-scatter.5.cloned.1.call-start = ((), (), s32[]{:S(2)}) async-start(), calls=%async_computation.6 | async-start | bytes 1114112 | tf_op jit(solution)/shard_map/reduce_scatter | solution.py:161
Sparse Core Ops, SparseCore 0:
  86.7 14.3 all-reduce.1
  104.5 56.2 all-gather.1
  172.9 7.2 reduce-scatter.2
  182.5 79.9 reduce-scatter.4
where the time goes:
time: 272 us; the launch traced here: 271 us
  waiting for transfers between devices  150 us (55%)
  blocking collectives  45.3 us (17%)
  other arithmetic  25.9 us (10%)
  local copies, waits for them, and re-layouts  21.8 us (8%)
  between operations  14.3 us (5%)
  matrix products  9.75 us (4%)
  starting transfers between devices  3.67 us (1%)
    reduce_scatter x1, waiting for transfers between devices, shards(): branch = lax.psum_scatter(halved, 'ep', scatter_dimension=0, tiled=True)  65.7 us
    all_gather x1, waiting for transfers between devices, shards(): gathered = lax.all_gather(normed, 'ep', axis=0, tiled=True)  54.8 us
    all_gather x1, blocking collectives, shards(): lax.all_gather(y_out, 'ep', axis=0, tiled=True)  45.3 us
    psum x1, waiting for transfers between devices, shards(): lax.psum(partial_value.astype(jnp.bfloat16), 'tp').astype(jnp.float32)  14.5 us
    mul x1, other arithmetic, state_update(): (step_size[:, :, None] * x_heads)[:, :, :, None]  8.51 us
    reshape x1, local copies, waits for them, and re-layouts, state_update(): state = ssm_state.reshape(count, heads, HEAD_P, NSTATE)  7.89 us
    mul x1, local copies, waits for them, and re-layouts, state_update(): (step_size[:, :, None] * x_heads)[:, :, :, None]  7.88 us
    all_to_all x1, waiting for transfers between devices, shards(): lax.all_to_all(partial_value.astype(jnp.bfloat16), 'ep', split_axis=0, co...  7.45 us
  transfers between devices with their start and end apart: 5, of which 5 were waited for; matrix products, arithmetic and copies ran while one was open for 6% of the time, Pallas kernels for 0%

commit v1 on v0

--- a/solution.py
+++ b/solution.py
@@ -90,7 +90,9 @@
         group_gain,
     )
     partial_value = jnp.dot(
-        lax.all_gather(y_out, "ep", axis=0, tiled=True),
+        jnp.concatenate(
+            lax.all_to_all(jnp.stack([y_out] * lax.axis_size("ep")), "ep", 0, 0), axis=0
+        ),
         out_proj,
         preferred_element_type=jnp.float32,
     )

time: 272 us -> 250 us (0.919)
  blocking collectives: 45.3 us -> 23.2 us
    all_gather x1 -> x0, blocking collectives: 45.3 us -> none  [shards(): lax.all_gather(y_out, 'ep', axis=0, tiled=True)]
    all_to_all x0 -> x1, blocking collectives: none -> 23.2 us  [shards(): lax.all_to_all(jnp.stack([y_out] * lax.axis_size('ep')), 'ep', 0, 0)]
  transfers between devices with their start and end apart: 5 -> 5, of which waited for: 5 -> 5; matrix products, arithmetic and copies ran while one was open for 6% -> 7% of each run, Pallas kernels for 0% -> 0%
where the time goes in v1:
time: 250 us; the launch traced here: 249 us
  waiting for transfers between devices  150 us (60%)
  other arithmetic  25.8 us (10%)
  blocking collectives  23.2 us (9%)
  local copies, waits for them, and re-layouts  21.9 us (9%)
  between operations  14.2 us (6%)
  matrix products  9.75 us (4%)
  starting transfers between devices  4.12 us (2%)
    reduce_scatter x1, waiting for transfers between devices, shards(): branch = lax.psum_scatter(halved, 'ep', scatter_dimension=0, tiled=True)  65.8 us
    all_gather x1, waiting for transfers between devices, shards(): gathered = lax.all_gather(normed, 'ep', axis=0, tiled=True)  54.8 us
    all_to_all x1, blocking collectives, shards(): lax.all_to_all(jnp.stack([y_out] * lax.axis_size('ep')), 'ep', 0, 0)  23.2 us
    psum x1, waiting for transfers between devices, shards(): lax.psum(partial_value.astype(jnp.bfloat16), 'tp').astype(jnp.float32)  14.6 us
    mul x1, other arithmetic, state_update(): (step_size[:, :, None] * x_heads)[:, :, :, None]  8.47 us
    reshape x1, local copies, waits for them, and re-layouts, state_update(): state = ssm_state.reshape(count, heads, HEAD_P, NSTATE)  7.89 us
    mul x1, local copies, waits for them, and re-layouts, state_update(): (step_size[:, :, None] * x_heads)[:, :, :, None]  7.88 us
    all_to_all x1, waiting for transfers between devices, shards(): lax.all_to_all(partial_value.astype(jnp.bfloat16), 'ep', split_axis=0, co...  7.48 us
  transfers between devices with their start and end apart: 5, of which 5 were waited for; matrix products, arithmetic and copies ran while one was open for 7% of the time, Pallas kernels for 0%

profile of v1, /device:TPU:0, one launch (start us, length us, event | category | flops | bytes accessed | tf_op | source)
XLA Modules:
  0.0 249.1 jit_solution(12635895204654175837)
XLA Ops:
  7.2 0.0 copy-start
  7.2 0.7 exp.39
  7.9 0.7 convert_element_type.90
  8.6 0.9 multiply_reduce_fusion.3
  9.6 0.1 reduce_sum.88
  9.7 0.7 convert_element_type.88
  10.4 0.9 multiply_reduce_fusion.1
  11.4 0.1 reduce_sum.86
  11.5 7.9 %reshape.184 = f32[16,16,64,64]{3,2,1,0:T(8,128)} reshape(f32[16,16,4096]{2,1,0:T(8,128)} %param.34) | data formatting | bytes 8388608 | tf_op jit(solution)/shard_map/reshape | solution.py:40
  19.4 0.1 multiply_multiply_fusion
  19.6 0.0 copy-start.5
  19.6 0.0 copy-start.7
  19.6 0.0 copy-start.4
  19.7 8.5 %broadcast_multiply_fusion = (f32[16,16,64,64]{3,2,1,0:T(8,128)}, f32[16,16,64]{2,1,0:T(8,128)S(1)}) fusion(f32[16,16,64]{2,1,0:T(8,128)S(1)} %bitcast.46, f32[16,16,64]{2,1,0:T(8,128)S(1)} %multiply_multiply_fusion, f32[16,16,64]{2,1,0:T(8,128)S(1)} %bitcast.47, f32[16,16,64,64]{3,2,1,0:T(8,128)} %reshape.184, f32[16,16]{1,0:T(8,128)S(1)} %get-tuple-element.11), kind=kLoop, calls=%fused_computation.3 | loop fusion | flops 5226496 | bytes 8651776 | tf_op jit(solution)/shard_map/mul | solution.py:41
  28.1 0.1 reshape.185
  28.3 0.1 reduce_sum.90
  28.4 0.1 mul.250
  28.6 0.1 stack.2
  28.7 23.2 %all_to_all.24 = bf16[16,16,1024]{2,1,0:T(8,128)(2,1)S(1)} all-to-all(bf16[16,16,1024]{2,1,0:T(8,128)(2,1)S(1)} %stack.2), channel_id=1, replica_groups=mesh['ep'=16,'tp'=2] {'ep'}, dimensions={0} | all-to-all | bytes 1048576 | tf_op jit(solution)/shard_map/all_to_all | solution.py:94
  51.9 0.9 convolution_convert_fusion.2
  52.8 4.0 %all-to-all-start.1 = ((bf16[16,16,128]{2,1,0:T(8,128)(2,1)}), bf16[16,16,128]{2,1,0:T(8,128)(2,1)S(1)}, u32[]{:S(2)}, u32[]{:S(2)}) async-start(bf16[16,16,128]{2,1,0:T(8,128)(2,1)} %bitcast.7), calls=%async_computation.1 | async-start | bytes 131072 | tf_op jit(solution)/shard_map/all_to_all | solution.py:99
  56.8 0.0 all-reduce.2.cloned.1.call-start
  56.8 7.5 %all-to-all-done.1 = bf16[16,16,128]{2,1,0:T(8,128)(2,1)S(1)} async-done(((bf16[16,16,128]{2,1,0:T(8,128)(2,1)}), bf16[16,16,128]{2,1,0:T(8,128)(2,1)S(1)}, u32[]{:S(2)}, u32[]{:S(2)}) %all-to-all-start.1) | async-done | bytes 65568 | tf_op jit(solution)/shard_map/all_to_all | solution.py:99
  64.3 0.6 copy_bitcast_fusion
  64.9 0.0 all-reduce.2.cloned.1.call-update
  65.0 0.0 all-gather.2.cloned.1.call-start
  65.0 14.6 %all-reduce.2.cloned.1.call-done = bf16[16,2048]{1,0:T(8,128)(2,1)} async-done(((bf16[16,2048]{1,0:T(8,128)(2,1)}), bf16[16,2048]{1,0:T(8,128)(2,1)}) %all-reduce.2.cloned.1.call-update) | async-done | bytes 65552 | tf_op jit(solution)/shard_map/psum | solution.py:102
  79.6 1.0 fusion.21
  80.6 1.6 multiply_convert_fusion
  82.1 0.0 all-gather.2.cloned.1.call-update
  82.2 0.0 reduce-scatter.3.cloned.1.call-start
  82.2 0.1 copy.39
  82.4 0.1 reshape.189
  82.5 0.3 reduce_window_sum.11
  82.7 0.4 select_reduce_fusion
  83.1 0.1 copy.40
  83.2 0.1 add.162
  83.3 0.1 add.159
  83.4 0.1 multiply_reduce_fusion.4
  83.5 0.1 copy.42
  83.7 0.1 mul.274
  83.8 0.2 fusion.26
  84.0 0.1 copy.43
  84.0 0.1 mul.277
  84.1 0.1 copy.41
  84.2 0.1 gt.18
  84.4 54.8 %all-gather.2.cloned.1.call-done = bf16[256,2048]{1,0:T(8,128)(2,1)} async-done(((bf16[16,2048]{1,0:T(8,128)(2,1)}), bf16[256,2048]{1,0:T(8,128)(2,1)}) %all-gather.2.cloned.1.call-update) | async-done | bytes 1048592 | tf_op jit(solution)/shard_map/all_gather | solution.py:110
  139.2 1.6 fusion.36
  140.9 2.8 %gather_fusion = bf16[112,2048]{1,0:T(8,128)(2,1)S(1)} fusion(bf16[256,2048]{1,0:T(8,128)(2,1)} %all-gather.2.cloned.1.call-done, s32[1024]{0:T(1024)S(1)} %pad_clamp_fusion), kind=kCustom, calls=%fused_computation | custom fusion | bytes 917952 | tf_op jit(solution)/shard_map/jit(_take)/gather | solution.py:139
  143.7 1.6 fusion.7
  145.3 0.6 convolution_convert_fusion.1
  145.9 0.5 fusion.37
  146.4 1.5 fusion.3
  148.0 0.2 copy.45
  148.2 3.0 %convolution_convert_fusion = bf16[256,2048]{1,0:T(8,128)(2,1)} fusion(bf16[256,384]{1,0:T(8,128)(2,1)S(1)} %bitcast.50, bf16[256,2048]{1,0:T(8,128)(2,1)} %bitcast.54, bf16[128,2048]{1,0:T(8,128)(2,1)} %param.42), kind=kOutput, calls=%fused_computation.4 | convolution fusion | flops 406323200 | bytes 2818048 | tf_op jit(solution)/shard_map/dot_general | solution.py:158
  151.2 0.0 reduce-scatter.3.cloned.1.call-update
  151.2 0.0 reduce-scatter.5.cloned.1.call-start
  151.3 7.3 %reduce-scatter.3.cloned.1.call-done = bf16[128,2048]{1,0:T(8,128)(2,1)} async-done(((bf16[256,2048]{1,0:T(8,128)(2,1)}), bf16[128,2048]{1,0:T(8,128)(2,1)}) %reduce-scatter.3.cloned.1.call-update) | async-done | bytes 524304 | tf_op jit(solution)/shard_map/reduce_scatter | solution.py:157
  158.6 2.2 convert_element_type.106
  160.8 0.0 reduce-scatter.5.cloned.1.call-update
  160.8 7.9 %mul.284 = f32[16,16,4096]{2,1,0:T(8,128)} reshape(f32[16,16,64,64]{3,2,1,0:T(8,128)} %get-tuple-element.4) | data formatting | bytes 8388608 | tf_op jit(solution)/shard_map/mul | solution.py:41
  168.7 6.6 %multiply_add_fusion = f32[16,16,4096]{2,1,0:T(8,128)} fusion(f32[16,16,4096]{2,1,0:T(8,128)} %mul.284, f32[16,16,4096]{2,1,0:T(8,128)} %param.34, f32[16,16]{1,0:T(8,128)S(1)} %get-tuple-element.11), kind=kLoop, calls=%fused_computation.2 | loop fusion | flops 2097152 | bytes 12583936 | tf_op jit(solution)/shard_map/add | solution.py:42
  175.3 65.8 %reduce-scatter.5.cloned.1.call-done = f32[8,2048]{1,0:T(8,128)} async-done(((f32[128,2048]{1,0:T(8,128)}), f32[8,2048]{1,0:T(8,128)}) %reduce-scatter.5.cloned.1.call-update) | async-done | bytes 65552 | tf_op jit(solution)/shard_map/reduce_scatter | solution.py:163
  241.1 1.5 add_convert_fusion.1
  (50 shorter events, 0.4 us)
Async XLA Ops:
  7.2 138.1 %copy-start = (bf16[1,2048,256]{2,1,0:T(8,128)(2,1)S(1)}, bf16[1,2048,256]{2,1,0:T(8,128)(2,1)}, u32[]{:S(2)}) copy-start(bf16[1,2048,256]{2,1,0:T(8,128)(2,1)} %param.48) | copy-start | bytes 3145732
  11.5 7.9 %copy-start.12 = (bf16[16,16]{1,0:T(8,128)(2,1)S(1)}, bf16[16,16]{1,0:T(8,128)(2,1)}, u32[]{:S(2)}) copy-start(bf16[16,16]{1,0:T(8,128)(2,1)} %param.29) | copy-start | bytes 1540
  11.5 7.9 %copy-start.13 = (f32[16]{0:T(128)S(1)}, f32[16]{0:T(128)}, u32[]{:S(2)}) copy-start(f32[16]{0:T(128)} %param.35) | copy-start | bytes 196
  19.6 8.7 %copy-start.5 = (bf16[16,1024]{1,0:T(8,128)(2,1)S(1)}, bf16[16,1024]{1,0:T(8,128)(2,1)}, u32[]{:S(2)}) copy-start(bf16[16,1024]{1,0:T(8,128)(2,1)} %param.27) | copy-start | bytes 98308
  19.6 8.9 %copy-start.9 = (f32[1024]{0:T(1024)S(1)}, f32[1024]{0:T(1024)}, u32[]{:S(2)}) copy-start(f32[1024]{0:T(1024)} %param.37) | copy-start | bytes 12292
  19.6 32.3 %copy-start.3 = (bf16[1024,128]{1,0:T(8,128)(2,1)S(1)}, bf16[1024,128]{1,0:T(8,128)(2,1)}, u32[]{:S(2)}) copy-start(bf16[1024,128]{1,0:T(8,128)(2,1)} %param.38) | copy-start | bytes 786436
  19.6 45.4 %copy-start.7 = (s32[256,6]{0,1:T(8,128)S(1)}, s32[256,6]{0,1:T(8,128)}, u32[]{:S(2)}) copy-start(s32[256,6]{0,1:T(8,128)} %param.45) | copy-start | bytes 18436
  19.6 60.0 %copy-start.4 = (bf16[16,2048]{1,0:T(8,128)(2,1)S(1)}, bf16[16,2048]{1,0:T(8,128)(2,1)}, u32[]{:S(2)}) copy-start(bf16[16,2048]{1,0:T(8,128)(2,1)} %param.25) | copy-start | bytes 196612
  19.6 60.9 %copy-start.6 = (f32[2048]{0:T(1024)S(1)}, f32[2048]{0:T(1024)}, u32[]{:S(2)}) copy-start(f32[2048]{0:T(1024)} %param.39) | copy-start | bytes 24580
  28.1 55.3 %copy-start.11 = (f32[256,4]{0,1:T(4,128)S(1)}, f32[256,4]{0,1:T(4,128)}, u32[]{:S(2)}) copy-start(f32[256,4]{0,1:T(4,128)} %param.44) | copy-start | bytes 12292
  28.1 55.4 %copy-start.8 = (f32[256,6]{0,1:T(8,128)S(1)}, f32[256,6]{0,1:T(8,128)}, u32[]{:S(2)}) copy-start(f32[256,6]{0,1:T(8,128)} %param.46) | copy-start | bytes 18436
  28.1 56.2 %copy-start.10 = (bf16[2048]{0:T(1024)(128)(2,1)S(1)}, bf16[2048]{0:T(1024)(128)(2,1)}, u32[]{:S(2)}) copy-start(bf16[2048]{0:T(1024)(128)(2,1)} %param.43) | copy-start | bytes 12292
  52.8 11.5 %all-to-all-start.1 = ((bf16[16,16,128]{2,1,0:T(8,128)(2,1)}), bf16[16,16,128]{2,1,0:T(8,128)(2,1)S(1)}, u32[]{:S(2)}, u32[]{:S(2)}) async-start(bf16[16,16,128]{2,1,0:T(8,128)(2,1)} %bitcast.7), calls=%async_computation.1 | async-start | bytes 131072 | tf_op jit(solution)/shard_map/all_to_all | solution.py:99
  56.8 22.8 %all-reduce.2.cloned.1.call-start = ((), (), s32[]{:S(2)}) async-start(), calls=%async_computation.4 | async-start | bytes 131072 | tf_op jit(solution)/shard_map/psum | solution.py:102
  65.0 74.3 %all-gather.2.cloned.1.call-start = ((), (), s32[]{:S(2)}) async-start(), calls=%async_computation.5 | async-start | bytes 1114112 | tf_op jit(solution)/shard_map/all_gather | solution.py:110
  82.2 76.4 %reduce-scatter.3.cloned.1.call-start = ((), (), s32[]{:S(2)}) async-start(), calls=%async_computation.6 | async-start | bytes 1572864 | tf_op jit(solution)/shard_map/reduce_scatter | solution.py:157
  140.8 5.0 %copy-start.1 = (bf16[256,2048]{1,0:T(8,128)(2,1)S(1)}, bf16[256,2048]{1,0:T(8,128)(2,1)}, u32[]{:S(2)}) copy-start(bf16[256,2048]{1,0:T(8,128)(2,1)} %all-gather.2.cloned.1.call-done) | copy-start | bytes 3145732
  140.8 5.1 %copy-start.2 = (bf16[2048,128]{1,0:T(8,128)(2,1)S(1)}, bf16[2048,128]{1,0:T(8,128)(2,1)}, u32[]{:S(2)}) copy-start(bf16[2048,128]{1,0:T(8,128)(2,1)} %param.40) | copy-start | bytes 1572868
  151.2 89.9 %reduce-scatter.5.cloned.1.call-start = ((), (), s32[]{:S(2)}) async-start(), calls=%async_computation.7 | async-start | bytes 1114112 | tf_op jit(solution)/shard_map/reduce_scatter | solution.py:163
Sparse Core Ops, SparseCore 0:
  65.1 14.4 all-reduce.1
  82.9 56.2 all-gather.1
  151.3 7.2 reduce-scatter.2
  161.0 80.0 reduce-scatter.4
